TPU v7x, 512 devices: a whole 4x8x8 slice. The times are simulated.
512 devices in a mesh: ep: 32 (over z, x), tp: 16 (over y, core).
Axes of the slice: x: 4, y: 8, z: 8, core: 2. Of those that a mesh axis runs over, the one named last changes fastest.
Arguments:
- queries: bfloat16 [4096, 512], P('ep'), may hold values from -6 to 6
- key_vectors: bfloat16 [4096, 512], P('ep'), may hold values from -6 to 6
- values: bfloat16 [4096, 1024], P('ep', 'tp'), may hold values from -6 to 6
- out_gate: bfloat16 [4096, 1024], P('ep', 'tp'), may hold values from -6 to 6
- input_gate: float32 [4096, 2], P('ep'), may hold values from -8 to 130
- forget_gate: float32 [4096, 2], P('ep'), may hold values from -2 to 16
- mix_weight: bfloat16 [1024, 2048], P('tp'), may hold values from -0.1875 to 0.1875
- expert_input: bfloat16 [8192, 2048], P('ep'), may hold values from -6 to 6
- norm_gain: float32 [2048], replicated, may hold values from 0.1 to 1.9
- route_ids: int32 [8192, 4], P('ep'), may hold values from 0 to 63, all different within a row; in each aligned block of 256 rows (0 to 255, 256 to 511, ...) at most 32 rows name the same one
- route_weights: float32 [8192, 4], P('ep'), may hold values from 0.2 to 1.2
- expert_gate: bfloat16 [512, 2048, 128], P(('ep', 'tp')), may hold values from -0.125 to 0.125
- expert_up: bfloat16 [512, 2048, 128], P(('ep', 'tp')), may hold values from -0.125 to 0.125
- expert_down: bfloat16 [512, 128, 2048], P(('ep', 'tp')), may hold values from -0.1875 to 0.1875
- shared_gate: bfloat16 [2048, 512], P(None, 'tp'), may hold values from -0.125 to 0.125
- shared_up: bfloat16 [2048, 512], P(None, 'tp'), may hold values from -0.125 to 0.125
- shared_down: bfloat16 [512, 2048], P('tp'), may hold values from -0.25 to 0.25
Outputs:
- mixer_out: bfloat16 [4096, 2048], P('ep')
- expert_out: bfloat16 [8192, 2048], P('ep')
Inputs may be any that keep to these rules, and one draw needn't show every extreme that they name: `route_ids`: each row names 4 different experts. In each aligned block of 256 rows (the rows of one index of ep) no expert is named by more than 32 rows, and in some block one expert is named by exactly 32 rows.
All inputs are finite; a program needn't handle non-finite values.
Results may differ from a plain program's by a relative error of at most 0.01575.
Values may be sent and summed in bfloat16 or wider, within the bound.
A program may use at most 64 MiB of HBM per device.

v0:
```python
import jax
import jax.numpy as jnp
from jax import lax
from jax.sharding import Mesh
from jax.sharding import PartitionSpec as P

D = 2048
MEMORY_HEADS = 2
KEY_DIM = 256
BLOCK = 128
FF = 1024
EP = ("ep_0", "ep_1")
EP_TP = ("ep_0", "ep_1", "tp")


epsilon = 1e-06
lowest = -1e30
den_floor = 4.0


def nothing_yet(array, identity):
    return jax.tree.map(
        lambda part, zero: jnp.zeros_like(part) + jnp.asarray(zero, part.dtype), array, identity
    )


def all_in_one(array, axis):
    leaves = jax.tree.leaves(array)
    order = sorted(range(len(leaves)), key=lambda k: -leaves[k].size)
    width = (1, *leaves[order[0]].shape)[-1]
    lines = [
        jnp.pad(leaves[k].reshape(-1), (0, -leaves[k].size % width)).reshape(-1, width)
        for k in order
    ]
    both, at, found = (lax.all_gather(jnp.concatenate(lines), axis), 0, {})
    for k, line in zip(order, lines):
        section = both[:, at : at + len(line)].reshape(len(both), -1)
        found[k] = section[:, : leaves[k].size].reshape(-1, *leaves[k].shape)
        at += len(line)
    numbers = iter(range(len(leaves)))
    return jax.tree.map(lambda _: found[next(numbers)], array)


def entering_2(array, axes, combine, identity):
    before = start = nothing_yet(array, identity)
    subtotal = array
    for axis in reversed(axes):
        count, place = (lax.axis_size(axis), lax.axis_index(axis))
        pieces = all_in_one(subtotal, axis)
        inside, subtotal = (start, start)
        for k in range(count):
            passed = k < place
            subtotal = combine(subtotal, jax.tree.map(lambda part: part[k], pieces))
            inside = jax.tree.map(lambda new, old: jnp.where(passed, new, old), subtotal, inside)
        before = combine(inside, before)
    return before


def in_blocks(array, dim, count):
    before, after = (array.shape[:dim], array.shape[dim + 1 :])
    return jnp.moveaxis(array.reshape(*before, count, -1, *after), dim, 0)


def summed_on_arrival(array, axis, dim):
    blocks = in_blocks(array, dim, lax.axis_size(axis))
    arrived = lax.all_to_all(blocks, axis, split_axis=0, concat_axis=0, tiled=True)
    return arrived.astype(jnp.float32).sum(axis=0)


def from_everyone(array, axis):
    copies = jnp.broadcast_to(array, (lax.axis_size(axis), *array.shape))
    return lax.all_to_all(copies, axis, split_axis=0, concat_axis=0, tiled=True)


def in_order(blocks, dim):
    blocks = jnp.moveaxis(blocks, 0, dim)
    shape = blocks.shape
    return blocks.reshape(*shape[:dim], shape[dim] * shape[dim + 1], *shape[dim + 2 :])


def collect(array, axis, dim):
    blocks = from_everyone(array, axis)
    return in_order(blocks, dim)


def combine_segments(earlier, later):
    first_decay, first_memory, first_normalizer, first_running = earlier
    second_decay, second_memory, second_normalizer, second_running = later
    running = jnp.maximum(second_decay + first_running, second_running)
    lead_scale = jnp.exp(second_decay + first_running - running)
    tail_scale = jnp.exp(second_running - running)
    return (
        first_decay + second_decay,
        lead_scale * first_memory + tail_scale * second_memory,
        lead_scale * first_normalizer + tail_scale * second_normalizer,
        running,
    )


def mixer_half(queries, key_vectors, values, out_gate, input_gate, forget_gate, mix_weight):
    tp_count = lax.axis_size("tp")
    tp_rank = lax.axis_index("tp")
    length = queries.shape[0]
    blocks = length // BLOCK
    channels = values.shape[1]
    factor = KEY_DIM ** (-0.5)
    head_index = tp_rank // (tp_count // MEMORY_HEADS)
    offset = head_index * KEY_DIM
    query_head = lax.dynamic_slice_in_dim(queries, offset, KEY_DIM, 1).reshape(
        blocks, BLOCK, KEY_DIM
    )
    key_head = lax.dynamic_slice_in_dim(key_vectors, offset, KEY_DIM, 1).reshape(
        blocks, BLOCK, KEY_DIM
    )
    value_blocks = values.reshape(blocks, BLOCK, channels)
    select = jnp.arange(MEMORY_HEADS, dtype=jnp.int32)[None, :] == head_index
    input_head = jnp.sum(jnp.where(select, input_gate, 0.0), axis=1).reshape(blocks, BLOCK)
    forget_head = jax.nn.log_sigmoid(jnp.sum(jnp.where(select, forget_gate, 0.0), axis=1)).reshape(
        blocks, BLOCK
    )
    cumulative = jnp.cumsum(forget_head, axis=1)
    block_total = cumulative[:, -1]
    log_retention = block_total[:, None] - cumulative + input_head
    block_running = jnp.max(log_retention, axis=1)
    weighted_keys = (
        key_head.astype(jnp.float32) * jnp.exp(log_retention - block_running[:, None])[:, :, None]
    )
    block_memory = jnp.einsum(
        "bsd,bsv->bdv",
        weighted_keys,
        value_blocks.astype(jnp.float32),
        precision=lax.Precision.HIGHEST,
    )
    block_normalizer = jnp.sum(weighted_keys, axis=1)
    segments = (block_total, block_memory, block_normalizer, block_running)
    neutral = (
        jnp.zeros((), jnp.float32),
        jnp.zeros((KEY_DIM, channels), jnp.float32),
        jnp.zeros((KEY_DIM,), jnp.float32),
        jnp.full((), lowest, jnp.float32),
    )

    def fold_block(carry_in, segment):
        return (combine_segments(carry_in, segment), None)

    summary, _ = lax.scan(fold_block, neutral, segments)
    prefix = entering_2(summary, EP, combine_segments, neutral)
    start_state = (
        jnp.zeros((), jnp.float32),
        jnp.zeros((KEY_DIM, channels), jnp.float32),
        jnp.zeros((KEY_DIM,), jnp.float32),
        jnp.zeros((), jnp.float32),
    )
    entering = combine_segments(start_state, prefix)
    causal = jnp.tril(jnp.ones((BLOCK, BLOCK), dtype=bool))

    def block_pass(carry_in, inputs):
        query_block, key_block, value_block, input_block, cumulative_block, segment = inputs
        _, memory, normalizer, running = carry_in
        carried = cumulative_block + running
        log_weight = cumulative_block[:, None] - cumulative_block[None, :] + input_block[None, :]
        log_weight = jnp.where(causal, log_weight, -jnp.inf)
        stabilizer = jnp.maximum(carried, jnp.max(log_weight, axis=1))
        within = jnp.exp(log_weight - stabilizer[:, None])
        across = jnp.exp(carried - stabilizer)
        scores = (
            jnp.einsum("td,sd->ts", query_block, key_block, preferred_element_type=jnp.float32)
            * factor
        )
        weights = scores * within
        scaled = query_block.astype(jnp.float32) * factor
        numerator = across[:, None] * jnp.dot(scaled, memory, precision=lax.Precision.HIGHEST)
        numerator = numerator + jnp.dot(
            weights.astype(jnp.bfloat16), value_block, preferred_element_type=jnp.float32
        )
        denominator = across * jnp.dot(scaled, normalizer, precision=lax.Precision.HIGHEST)
        denominator = denominator + jnp.sum(weights, axis=1)
        hidden = numerator / jnp.maximum(jnp.abs(denominator), den_floor)[:, None]
        return (combine_segments(carry_in, segment), hidden)

    _, hidden = lax.scan(
        block_pass, entering, (query_head, key_head, value_blocks, input_head, cumulative, segments)
    )
    gated_rows = (
        hidden.reshape(length, channels) * jax.nn.sigmoid(out_gate.astype(jnp.float32))
    ).astype(jnp.bfloat16)
    return jnp.dot(gated_rows, mix_weight, preferred_element_type=jnp.float32)


def expert_half(
    expert_input,
    norm_gain,
    route_ids,
    route_weights,
    expert_gate,
    expert_up,
    expert_down,
    shared_gate,
    shared_up,
    shared_down,
):
    ep_count = lax.axis_size(EP)
    tp_count = lax.axis_size("tp")
    tp_rank = lax.axis_index("tp")
    tokens = expert_input.shape[0]
    top_count = route_ids.shape[1]
    slice_units = expert_gate.shape[2]
    group_size = FF // slice_units
    per_ep = tp_count // group_size
    team_index = tp_rank // group_size
    expert_count = ep_count * per_ep
    capacity = 2 * tokens * top_count // expert_count
    rows_wide = expert_input.astype(jnp.float32)
    normed = (
        rows_wide
        * lax.rsqrt(jnp.mean(rows_wide * rows_wide, axis=-1, keepdims=True) + epsilon)
        * norm_gain
    ).astype(jnp.bfloat16)
    chosen = route_ids.reshape(-1)
    onehot = (chosen[:, None] == jnp.arange(expert_count, dtype=jnp.int32)[None, :]).astype(
        jnp.int32
    )
    slot_rank = jnp.sum((jnp.cumsum(onehot, axis=0) - onehot) * onehot, axis=1)
    in_team = chosen % per_ep == team_index
    target = jnp.where(in_team, chosen // per_ep * capacity + slot_rank, ep_count * capacity)
    token_of = jnp.arange(chosen.shape[0], dtype=jnp.int32) // top_count
    slot_token = jnp.zeros((ep_count * capacity,), jnp.int32).at[target].set(token_of, mode="drop")
    slot_live = jnp.zeros((ep_count * capacity,), jnp.int32).at[target].set(1, mode="drop")
    outgoing = jnp.where(slot_live[:, None] > 0, normed[slot_token], jnp.zeros((), jnp.bfloat16))
    outgoing = outgoing.reshape(ep_count, capacity, D)
    gate_slice = expert_gate[0]
    up_slice = expert_up[0]
    down_slice = expert_down[0]
    arrived = lax.all_to_all(outgoing, EP, split_axis=0, concat_axis=0, tiled=True)
    gate_val = jnp.einsum("sid,df->sif", arrived, gate_slice, preferred_element_type=jnp.float32)
    up_val = jnp.einsum("sid,df->sif", arrived, up_slice, preferred_element_type=jnp.float32)
    hidden = (jax.nn.silu(gate_val) * up_val).astype(jnp.bfloat16)
    partial_value = jnp.einsum(
        "sif,fd->sid", hidden, down_slice, preferred_element_type=jnp.float32
    )
    partial_value = partial_value.astype(jnp.bfloat16)
    returned = lax.all_to_all(partial_value, EP, split_axis=0, concat_axis=0, tiled=True)
    flat_back = returned.reshape(ep_count * capacity, returned.shape[2])
    gather_at = jnp.where(in_team, target, 0).reshape(tokens, top_count)
    weight_at = jnp.where(in_team, route_weights.reshape(-1), 0.0).reshape(tokens, top_count)
    combined = jnp.zeros((tokens, returned.shape[2]), jnp.float32)
    for pick_index in range(top_count):
        combined = (
            combined
            + flat_back[gather_at[:, pick_index]].astype(jnp.float32)
            * weight_at[:, pick_index][:, None]
        )
    shared_gate_val = jnp.dot(normed, shared_gate, preferred_element_type=jnp.float32)
    shared_up_val = jnp.dot(normed, shared_up, preferred_element_type=jnp.float32)
    shared_act = (jax.nn.silu(shared_gate_val) * shared_up_val).astype(jnp.bfloat16)
    return combined + jnp.dot(shared_act, shared_down, preferred_element_type=jnp.float32)


def shards(
    queries,
    key_vectors,
    values,
    out_gate,
    input_gate,
    forget_gate,
    mix_weight,
    expert_input,
    norm_gain,
    route_ids,
    route_weights,
    expert_gate,
    expert_up,
    expert_down,
    shared_gate,
    shared_up,
    shared_down,
):
    mixer_partial = mixer_half(
        queries, key_vectors, values, out_gate, input_gate, forget_gate, mix_weight
    )
    expert_partial = expert_half(
        expert_input,
        norm_gain,
        route_ids,
        route_weights,
        expert_gate,
        expert_up,
        expert_down,
        shared_gate,
        shared_up,
        shared_down,
    )
    mixer_piece = summed_on_arrival(mixer_partial.astype(jnp.bfloat16), "tp", 0).astype(
        jnp.bfloat16
    )
    mixer_out = lax.all_gather(mixer_piece, "tp", axis=0, tiled=True)
    expert_piece = lax.psum_scatter(expert_partial, "tp", scatter_dimension=0, tiled=True).astype(
        jnp.bfloat16
    )
    expert_out = collect(expert_piece, "tp", 0)
    return (mixer_out, expert_out)


def solution(mesh):
    finer = Mesh(mesh.devices.reshape(8, 4, mesh.shape["tp"]), ("ep_0", "ep_1", "tp"))
    placed = (
        P(EP, None),
        P(EP, None),
        P(EP, "tp"),
        P(EP, "tp"),
        P(EP, None),
        P(EP, None),
        P("tp", None),
        P(EP, None),
        P(),
        P(EP, None),
        P(EP, None),
        P(EP_TP, None, None),
        P(EP_TP, None, None),
        P(EP_TP, None, None),
        P(None, "tp"),
        P(None, "tp"),
        P("tp", None),
    )
    return jax.shard_map(
        shards, mesh=finer, in_specs=placed, out_specs=(P(EP, None), P(EP, None)), check_vma=False
    )
```

profile of v0, /device:TPU:1, one launch (start us, length us, event | category | flops | bytes accessed | tf_op | source)
XLA Modules:
  0.0 426.6 jit_solution(15270256443497055373)
XLA Ops:
  7.2 0.9 copy.108
  8.6 18.0 %reduce-window.6 = s32[64,8,128]{2,1,0:T(8,128)S(1)} reduce-window(s32[64,8,128]{2,1,0:T(8,128)S(1)} %fusion.29, s32[]{:T(128)} %constant.140.clone.1), window={size=1x1x128 pad=0_0x0_0x127_0}, to_apply=%region_8.9 | reduce-window | flops 8323072 | bytes 524292 | tf_op jit(solution)/shard_map/reduce-window
  27.3 4.3 %scatter_custom_fusion.1 = s32[1024]{0:T(1024)S(1)} fusion(s32[1024]{0:T(1024)S(1)} %bitcast.173, s32[1024]{0:T(1024)S(1)} %add_select_fusion.3, s32[]{:T(128)} %constant.140.clone.1), kind=kCustom, calls=%fused_computation.234 | custom fusion | bytes 4100 | tf_op jit(solution)/shard_map/scatter | solution.py:227
  31.9 4.3 %scatter_custom_fusion = s32[1024]{0:T(1024)S(1)} fusion(s32[1024]{0:T(1024)S(1)} %bitcast.174, s32[1024]{0:T(1024)S(1)} %broadcast.491, s32[]{:T(128)} %constant.140.clone.1), kind=kCustom, calls=%fused_computation.237 | custom fusion | bytes 4100 | tf_op jit(solution)/shard_map/scatter | solution.py:228
  36.6 6.0 %gather_fusion = bf16[1024,2048]{1,0:T(8,128)(2,1)} fusion(bf16[256,2048]{1,0:T(8,128)(2,1)S(1)} %fusion.3, s32[1024]{0:T(1024)S(1)} %fusion.157), kind=kCustom, calls=%fused_computation | custom fusion | bytes 8392704 | tf_op jit(solution)/shard_map/gather | solution.py:229
  42.7 2.5 broadcast_select_fusion
  45.2 107.2 %all_to_all.20 = bf16[32,32,2048]{2,1,0:T(8,128)(2,1)S(1)} all-to-all(bf16[32,32,2048]{2,1,0:T(8,128)(2,1)S(1)} %broadcast_select_fusion), channel_id=1, replica_groups=mesh['ep_0'=8,'ep_1'=4,'tp'=16] {'ep_0','ep_1'}, dimensions={0} | all-to-all | bytes 8388608 | tf_op jit(solution)/shard_map/all_to_all | solution.py:234
  152.5 1.9 copy-done.1
  154.4 1.2 fusion.18
  155.7 8.5 %convolution_convert_fusion = bf16[32,32,2048]{2,1,0:T(8,128)(2,1)} fusion(bf16[32,32,2048]{2,1,0:T(8,128)(2,1)} %copy-done.1, bf16[1,128,2048]{2,1,0:T(8,128)(2,1)S(1)} %copy-done, bf16[1,2048,128]{2,1,0:T(8,128)(2,1)S(1)} %copy-done.4, f32[32,32,128]{2,1,0:T(8,128)S(1)} %fusion.18), kind=kOutput, calls=%fused_computation.8 | convolution fusion | flops 1076625408 | bytes 9961472 | tf_op jit(solution)/shard_map/sif,fd->sid/dot_general | solution.py:238
  164.2 6.7 %all-to-all-start.2 = ((bf16[32,32,2048]{2,1,0:T(8,128)(2,1)}), bf16[32,32,2048]{2,1,0:T(8,128)(2,1)}, u32[]{:S(2)}, u32[]{:S(2)}) async-start(bf16[32,32,2048]{2,1,0:T(8,128)(2,1)} %convolution_convert_fusion), calls=%async_computation.2 | async-start | bytes 8388608 | tf_op jit(solution)/shard_map/all_to_all | solution.py:242
  172.7 1.2 fusion.178
  175.4 1.3 subtract_exponential_fusion.1
  178.2 20.0 %all-gather.2 = f32[4,262,64]{1,2,0:T(8,128)S(1)} all-gather(f32[1,262,64]{1,2,0:T(8,128)S(1)} %maximum_bitcast_fusion), channel_id=2, replica_groups=mesh['ep_0'=8,'ep_1'=4,'tp'=16] {'ep_1'}, dimensions={0}, use_global_device_ids=true | all-gather | bytes 335360 | tf_op jit(solution)/shard_map/all_gather | solution.py:35
  211.3 0.7 copy.96
  213.8 0.9 slice_reduce_fusion.3
  215.1 48.3 %all-to-all-done.2 = bf16[32,32,2048]{2,1,0:T(8,128)(2,1)} async-done(((bf16[32,32,2048]{2,1,0:T(8,128)(2,1)}), bf16[32,32,2048]{2,1,0:T(8,128)(2,1)}, u32[]{:S(2)}, u32[]{:S(2)}) %all-to-all-start.2) | async-done | bytes 4194336 | tf_op jit(solution)/shard_map/all_to_all | solution.py:242
  263.5 5.2 %gather_fusion.1 = bf16[256,2048]{1,0:T(8,128)(2,1)S(1)} fusion(bf16[1024,2048]{1,0:T(8,128)(2,1)} %bitcast.58, s32[1024]{0:T(1024)} %get-tuple-element.135), kind=kCustom, calls=%fused_computation.1 | custom fusion | bytes 2098176 | tf_op jit(solution)/shard_map/gather | solution.py:250
  268.7 6.2 %gather_fusion.2 = bf16[256,2048]{1,0:T(8,128)(2,1)} fusion(bf16[1024,2048]{1,0:T(8,128)(2,1)} %bitcast.58, s32[1024]{0:T(1024)} %get-tuple-element.134), kind=kCustom, calls=%fused_computation.2 | custom fusion | bytes 2098176 | tf_op jit(solution)/shard_map/gather | solution.py:250
  274.9 6.2 %gather_fusion.3 = bf16[256,2048]{1,0:T(8,128)(2,1)} fusion(bf16[1024,2048]{1,0:T(8,128)(2,1)} %bitcast.58, s32[1024]{0:T(1024)} %get-tuple-element.133), kind=kCustom, calls=%fused_computation.3 | custom fusion | bytes 2098176 | tf_op jit(solution)/shard_map/gather | solution.py:250
  281.2 6.2 %gather_fusion.4 = bf16[256,2048]{1,0:T(8,128)(2,1)} fusion(bf16[1024,2048]{1,0:T(8,128)(2,1)} %bitcast.58, s32[1024]{0:T(1024)} %get-tuple-element.132), kind=kCustom, calls=%fused_computation.4 | custom fusion | bytes 2098176 | tf_op jit(solution)/shard_map/gather | solution.py:250
  287.4 5.0 %convolution_add_fusion = f32[256,2048]{1,0:T(8,128)} fusion(bf16[32,2048]{1,0:T(8,128)(2,1)S(1)} %copy-done.6, bf16[256,2048]{1,0:T(8,128)(2,1)} %gather_fusion.4, bf16[256,2048]{1,0:T(8,128)(2,1)} %gather_fusion.3, bf16[256,2048]{1,0:T(8,128)(2,1)} %gather_fusion.2, bf16[256,2048]{1,0:T(8,128)(2,1)S(1)} %gather_fusion.1, bf16[256,2048]{1,0:T(8,128)(2,1)S(1)} %fusion.3, ...), kind=kOutput, calls=%fused_computation.9 | convolution fusion | flops 73449472 | bytes 7639040 | tf_op jit(solution)/shard_map/dot_general | solution.py:256
  293.3 21.1 %all-gather.3 = f32[8,262,64]{1,2,0:T(8,128)S(1)} all-gather(f32[1,262,64]{1,2,0:T(8,128)S(1)} %maximum_bitcast_fusion.1), channel_id=3, replica_groups=mesh['ep_0'=8,'ep_1'=4,'tp'=16] {'ep_0'}, dimensions={0}, use_global_device_ids=true | all-gather | bytes 603648 | tf_op jit(solution)/shard_map/all_gather | solution.py:35
  340.8 1.3 fusion
  342.1 16.0 %all-to-all-start = ((bf16[16,8,2048]{2,1,0:T(8,128)(2,1)}), bf16[16,8,2048]{2,1,0:T(8,128)(2,1)S(1)}, u32[]{:S(2)}, u32[]{:S(2)}) async-start(bf16[16,8,2048]{2,1,0:T(8,128)(2,1)} %fusion), calls=%async_computation | async-start | bytes 1048576 | tf_op jit(solution)/shard_map/all_to_all | solution.py:66
  358.1 0.9 convert_element_type.83
  359.0 16.3 %all-to-all-done = bf16[16,8,2048]{2,1,0:T(8,128)(2,1)S(1)} async-done(((bf16[16,8,2048]{2,1,0:T(8,128)(2,1)}), bf16[16,8,2048]{2,1,0:T(8,128)(2,1)S(1)}, u32[]{:S(2)}, u32[]{:S(2)}) %all-to-all-start) | async-done | bytes 524320 | tf_op jit(solution)/shard_map/all_to_all | solution.py:66
  375.3 1.1 broadcast_in_dim.93
  376.4 3.6 all-to-all-start.3
  380.0 37.9 %all_gather.19 = bf16[128,2048]{1,0:T(8,128)(2,1)S(1)} all-gather(bf16[8,2048]{1,0:T(8,128)(2,1)S(1)} %reduce_sum.75), channel_id=1, replica_groups=mesh['ep_0'=8,'ep_1'=4,'tp'=16] {'tp'}, dimensions={0}, use_global_device_ids=true | all-gather | bytes 557056 | tf_op jit(solution)/shard_map/all_gather | solution.py:296
  418.0 0.8 copy.149
  418.8 1.0 copy.150
  (151 shorter events, 13.9 us)
Async XLA Ops:
  7.2 148.5 %copy-start = (bf16[1,128,2048]{2,1,0:T(8,128)(2,1)S(1)}, bf16[1,128,2048]{2,1,0:T(8,128)(2,1)}, u32[]{:S(2)}) copy-start(bf16[1,128,2048]{2,1,0:T(8,128)(2,1)} %param.30) | copy-start | bytes 1572868
  7.2 24.4 %copy-start.2 = (bf16[256,2048]{1,0:T(8,128)(2,1)S(1)}, bf16[256,2048]{1,0:T(8,128)(2,1)}, u32[]{:S(2)}) copy-start(bf16[256,2048]{1,0:T(8,128)(2,1)} %param.24) | copy-start | bytes 3145732
  7.2 29.1 %copy-start.25 = (f32[2048]{0:T(1024)S(1)}, f32[2048]{0:T(1024)}, u32[]{:S(2)}) copy-start(f32[2048]{0:T(1024)} %param.25) | copy-start | bytes 24580
  45.2 109.2 %copy-start.3 = (bf16[1,2048,128]{2,1,0:T(8,128)(2,1)S(1)}, bf16[1,2048,128]{2,1,0:T(8,128)(2,1)}, u32[]{:S(2)}) copy-start(bf16[1,2048,128]{2,1,0:T(8,128)(2,1)} %param.28) | copy-start | bytes 1572868
  152.5 1.9 copy-start.1
  154.4 1.3 copy-start.4
  164.2 6.9 %copy-start.29 = (f32[128,2]{0,1:T(2,128)S(1)}, f32[128,2]{0,1:T(2,128)}, u32[]{:S(2)}) copy-start(f32[128,2]{0,1:T(2,128)} %param.21) | copy-start | bytes 3076
  164.2 6.9 %copy-start.30 = (f32[128,2]{0,1:T(2,128)S(1)}, f32[128,2]{0,1:T(2,128)}, u32[]{:S(2)}) copy-start(f32[128,2]{0,1:T(2,128)} %param.22) | copy-start | bytes 3076
  164.2 12.5 %copy-start.9 = (bf16[128,512]{1,0:T(8,128)(2,1)S(1)}, bf16[128,512]{1,0:T(8,128)(2,1)}, u32[]{:S(2)}) copy-start(bf16[128,512]{1,0:T(8,128)(2,1)} %param.18) | copy-start | bytes 393220
  164.2 13.7 %copy-start.11 = (bf16[128,64]{0,1:T(8,128)(2,1)S(1)}, bf16[128,64]{0,1:T(8,128)(2,1)}, u32[]{:S(2)}) copy-start(bf16[128,64]{0,1:T(8,128)(2,1)} %param.19) | copy-start | bytes 49156
  164.2 43.6 %copy-start.22 = (s32[256,4]{0,1:T(4,128)S(1)}, s32[256,4]{0,1:T(4,128)}, u32[]{:S(2)}) copy-start(s32[256,4]{0,1:T(4,128)} %param.26) | copy-start | bytes 12292
  164.2 43.8 %copy-start.28 = (f32[256,4]{0,1:T(4,128)S(1)}, f32[256,4]{0,1:T(4,128)}, u32[]{:S(2)}) copy-start(f32[256,4]{0,1:T(4,128)} %param.27) | copy-start | bytes 12292
  164.2 99.3 %all-to-all-start.2 = ((bf16[32,32,2048]{2,1,0:T(8,128)(2,1)}), bf16[32,32,2048]{2,1,0:T(8,128)(2,1)}, u32[]{:S(2)}, u32[]{:S(2)}) async-start(bf16[32,32,2048]{2,1,0:T(8,128)(2,1)} %convolution_convert_fusion), calls=%async_computation.2 | async-start | bytes 8388608 | tf_op jit(solution)/shard_map/all_to_all | solution.py:242
  170.9 187.2 %reduce-scatter.2.cloned.1.call-start = ((), (), s32[]{:S(2)}) async-start(), calls=%async_computation.5 | async-start | bytes 2228224 | tf_op jit(solution)/shard_map/reduce_scatter | solution.py:297
  171.2 5.6 %copy-start.26 = (f32[128]{0:T(128)}, f32[128]{0:T(128)S(1)}, u32[]{:S(2)}) copy-start(f32[128]{0:T(128)S(1)} %get-tuple-element.69) | copy-start | bytes 1540
  171.5 37.0 %copy-start.23 = (f32[1,128]{1,0:T(1,128)}, f32[1,128]{1,0:T(1,128)S(1)}, u32[]{:S(2)}) copy-start(f32[1,128]{1,0:T(1,128)S(1)} %reduce_window_sum.26) | copy-start | bytes 1540
  177.9 36.9 %copy-start.8 = (bf16[2048,32]{0,1:T(8,128)(2,1)S(1)}, bf16[2048,32]{0,1:T(8,128)(2,1)}, u32[]{:S(2)}) copy-start(bf16[2048,32]{0,1:T(8,128)(2,1)} %param.31) | copy-start | bytes 393220
  208.7 0.6 copy-start.15
  281.2 6.2 %copy-start.6 = (bf16[32,2048]{1,0:T(8,128)(2,1)S(1)}, bf16[32,2048]{1,0:T(8,128)(2,1)}, u32[]{:S(2)}) copy-start(bf16[32,2048]{1,0:T(8,128)(2,1)} %param.33) | copy-start | bytes 393220
  281.2 6.2 %copy-start.7 = (bf16[2048,32]{0,1:T(8,128)(2,1)S(1)}, bf16[2048,32]{0,1:T(8,128)(2,1)}, u32[]{:S(2)}) copy-start(bf16[2048,32]{0,1:T(8,128)(2,1)} %param.32) | copy-start | bytes 393220
  292.4 0.8 copy-start.10
  292.5 47.1 %copy-start.14 = (f32[1,4,64]{2,1,0:T(4,128)S(1)}, f32[1,4,64]{2,1,0:T(4,128)}, u32[]{:S(2)}) copy-start(f32[1,4,64]{2,1,0:T(4,128)} %copy-done.13) | copy-start | bytes 3076
  292.5 47.1 %copy-start.16 = (f32[1,4,64]{2,1,0:T(4,128)S(1)}, f32[1,4,64]{2,1,0:T(4,128)}, u32[]{:S(2)}) copy-start(f32[1,4,64]{2,1,0:T(4,128)} %copy-done.15) | copy-start | bytes 3076
  292.5 47.1 %copy-start.18 = (f32[1,4,64]{2,1,0:T(4,128)S(1)}, f32[1,4,64]{2,1,0:T(4,128)}, u32[]{:S(2)}) copy-start(f32[1,4,64]{2,1,0:T(4,128)} %copy-done.17) | copy-start | bytes 3076
  292.5 47.1 %copy-start.20 = (f32[1,4,64]{2,1,0:T(4,128)S(1)}, f32[1,4,64]{2,1,0:T(4,128)}, u32[]{:S(2)}) copy-start(f32[1,4,64]{2,1,0:T(4,128)} %copy-done.19) | copy-start | bytes 3076
  292.5 47.3 %copy-start.24 = (f32[1,128]{1,0:T(1,128)S(1)}, f32[1,128]{1,0:T(1,128)}, u32[]{:S(2)}) copy-start(f32[1,128]{1,0:T(1,128)} %copy-done.23) | copy-start | bytes 1540
  292.5 47.3 %copy-start.27 = (f32[128]{0:T(128)S(1)}, f32[128]{0:T(128)}, u32[]{:S(2)}) copy-start(f32[128]{0:T(128)} %copy-done.26) | copy-start | bytes 1540
  292.5 47.5 %copy-start.12 = (bf16[128,512]{1,0:T(8,128)(2,1)S(1)}, bf16[128,512]{1,0:T(8,128)(2,1)}, u32[]{:S(2)}) copy-start(bf16[128,512]{1,0:T(8,128)(2,1)} %param.17) | copy-start | bytes 393220
  314.3 26.5 %copy-start.5 = (bf16[64,2048]{1,0:T(8,128)(2,1)S(1)}, bf16[64,2048]{1,0:T(8,128)(2,1)}, u32[]{:S(2)}) copy-start(bf16[64,2048]{1,0:T(8,128)(2,1)} %param.23) | copy-start | bytes 786436
  314.4 26.5 %copy-start.21 = (bf16[128,64]{0,1:T(8,128)(2,1)S(1)}, bf16[128,64]{0,1:T(8,128)(2,1)}, u32[]{:S(2)}) copy-start(bf16[128,64]{0,1:T(8,128)(2,1)} %param.20) | copy-start | bytes 49156
  342.1 33.2 %all-to-all-start = ((bf16[16,8,2048]{2,1,0:T(8,128)(2,1)}), bf16[16,8,2048]{2,1,0:T(8,128)(2,1)S(1)}, u32[]{:S(2)}, u32[]{:S(2)}) async-start(bf16[16,8,2048]{2,1,0:T(8,128)(2,1)} %fusion), calls=%async_computation | async-start | bytes 1048576 | tf_op jit(solution)/shard_map/all_to_all | solution.py:66
  376.4 41.6 %all-to-all-start.3 = ((bf16[16,16,2048]{2,1,0:T(8,128)(2,1)}), bf16[16,16,2048]{2,1,0:T(8,128)(2,1)S(1)}, u32[]{:S(2)}, u32[]{:S(2)}) async-start(bf16[16,16,2048]{2,1,0:T(8,128)(2,1)} %broadcast_in_dim.93), calls=%async_computation.4 | async-start | bytes 2097152 | tf_op jit(solution)/shard_map/all_to_all | solution.py:72
  (3 other events, 1.8 us)
Sparse Core Ops, SparseCore 0:
  292.6 61.3 reduce-scatter.1
where the time goes:
time: 428 us; the launch traced here: 427 us
  blocking collectives  186 us (43%)
  waiting for transfers between devices  64.6 us (15%)
  local copies, waits for them, and re-layouts  54.5 us (13%)
  between operations  49.7 us (12%)
  other arithmetic  27.8 us (6%)
  starting transfers between devices  26.2 us (6%)
  matrix products  17.5 us (4%)
    all_to_all x1, blocking collectives, expert_half(): lax.all_to_all(outgoing, EP, split_axis=0, concat_axis=0, tiled=True)  107 us
    all_to_all x1, waiting for transfers between devices, expert_half(): lax.all_to_all(partial_value, EP, split_axis=0, concat_axis=0, tiled=True)  48.3 us
    all_gather x2, blocking collectives, all_in_one(): both, at, found = (lax.all_gather(jnp.concatenate(lines), axis), 0, {})  41.1 us
    all_gather x1, blocking collectives, shards(): mixer_out = lax.all_gather(mixer_piece, 'tp', axis=0, tiled=True)  37.9 us
    gather x4, local copies, waits for them, and re-layouts, expert_half(): flat_back[gather_at[:, pick_index]].astype(jnp.float32)  23.9 us
    another operation x3, other arithmetic  18.2 us
    all_to_all x1, waiting for transfers between devices, summed_on_arrival(): lax.all_to_all(blocks, axis, split_axis=0, concat_axis=0, tiled=True)  16.3 us
    all_to_all x1, starting transfers between devices, summed_on_arrival(): lax.all_to_all(blocks, axis, split_axis=0, concat_axis=0, tiled=True)  16 us
  transfers between devices with their start and end apart: 4, of which 2 were waited for; matrix products, arithmetic and copies ran while one was open for 4% of the time, Pallas kernels for 0%

commit v1 on v0

v1 whole, which is shorter than its diff:
```python
import functools

import jax
import jax.numpy as jnp
from jax import lax
from jax.experimental import pallas as pl
from jax.experimental.pallas import tpu as pltpu
from jax.sharding import Mesh
from jax.sharding import PartitionSpec as P

MEMORY_HEADS = 2
KEY_DIM = 256
CAP = 32
ROWS = CAP // 2
LANES = 128
EP = ("z", "x")
TP = ("y", "c")
MESH = pl.DeviceIdType.MESH

epsilon = 1e-06
lowest = -1e30
den_floor = 4.0


def mixer_local(queries, key_vectors, values, out_gate, input_gate, forget_gate, head):
    length = queries.shape[0]
    factor = KEY_DIM ** (-0.5)
    offset = head * KEY_DIM
    query = lax.dynamic_slice_in_dim(queries, offset, KEY_DIM, 1)
    key = lax.dynamic_slice_in_dim(key_vectors, offset, KEY_DIM, 1)
    select = jnp.arange(MEMORY_HEADS, dtype=jnp.int32)[None, :] == head
    gate_in = jnp.sum(jnp.where(select, input_gate, 0.0), axis=1)
    lf = jax.nn.log_sigmoid(jnp.sum(jnp.where(select, forget_gate, 0.0), axis=1))
    causal = jnp.tril(jnp.ones((length, length), dtype=bool))
    cumulative = jnp.sum(jnp.where(causal, lf[None, :], 0.0), axis=1)
    total = cumulative[length - 1]
    log_keep = total - cumulative + gate_in
    running = jnp.max(log_keep)
    weighted = key.astype(jnp.float32) * jnp.exp(log_keep - running)[:, None]
    memory_t = lax.dot_general(
        values.astype(jnp.float32),
        weighted,
        (((0,), (0,)), ((), ())),
        precision=lax.Precision.HIGHEST,
    )
    stats = jnp.concatenate(
        [
            jnp.sum(weighted, axis=0)[None, :],
            jnp.broadcast_to(total, (1, KEY_DIM)),
            jnp.broadcast_to(running, (1, KEY_DIM)),
            jnp.zeros((5, KEY_DIM), jnp.float32),
        ]
    )
    state = jnp.concatenate([memory_t, stats])
    log_weight = cumulative[:, None] - cumulative[None, :] + gate_in[None, :]
    log_weight = jnp.where(causal, log_weight, -jnp.inf)
    peak = jnp.max(log_weight, axis=1)
    scores = (
        lax.dot_general(
            query, key, (((1,), (1,)), ((), ())), preferred_element_type=jnp.float32
        )
        * factor
    )
    weights = scores * jnp.exp(log_weight - peak[:, None])
    inside_t = lax.dot_general(
        values,
        weights.astype(jnp.bfloat16),
        (((0,), (1,)), ((), ())),
        preferred_element_type=jnp.float32,
    )
    rows = jnp.concatenate(
        [
            cumulative[None, :],
            peak[None, :],
            jnp.sum(weights, axis=1)[None, :],
            jnp.zeros((5, length), jnp.float32),
        ]
    )
    gate_t = jax.nn.sigmoid(out_gate.astype(jnp.float32)).T
    scaled = query * jnp.asarray(factor, jnp.bfloat16)
    return state, rows, inside_t, gate_t, scaled


def routing(route_ids, route_weights, team, core, nz, nx):
    tokens, top = route_ids.shape
    count = nz * nx
    wanted = jnp.arange(count, dtype=jnp.int32)[None, :] * 2 + team
    named = jnp.zeros((tokens, count), jnp.float32)
    weight = jnp.zeros((tokens, count), jnp.float32)
    for k in range(top):
        hit = route_ids[:, k : k + 1] == wanted
        named = named + hit.astype(jnp.float32)
        weight = weight + jnp.where(hit, route_weights[:, k : k + 1], 0.0)
    earlier = jnp.tril(jnp.ones((tokens, tokens), jnp.bfloat16), -1)
    rank = jnp.dot(earlier, named.astype(jnp.bfloat16), preferred_element_type=jnp.float32)
    slot = jnp.where(named > 0, rank, -1.0).astype(jnp.int32) - core * ROWS
    by_dest = slot.reshape(tokens, nz, nx).transpose(2, 1, 0)
    weight_by = weight.reshape(tokens, nz, nx).transpose(2, 1, 0)
    own = jnp.arange(ROWS, dtype=jnp.int32)[None, None, :, None]
    hit = by_dest[:, :, None, :] == own
    pick = hit.astype(jnp.bfloat16).reshape(nx, nz * ROWS, tokens)
    spread = jnp.where(hit, weight_by[:, :, None, :], 0.0)
    high = lax.reduce_precision(spread, 8, 7)
    low = spread - high
    high = high.astype(jnp.bfloat16).reshape(nx, nz * ROWS, tokens)
    low = low.astype(jnp.bfloat16).reshape(nx, nz * ROWS, tokens)
    return pick, high, low


def kernel(
    nz,
    nx,
    ny,
    xh,
    pick,
    whi,
    wlo,
    gate_in,
    up_in,
    down_in,
    state,
    rows,
    inside,
    sig,
    scaled,
    mixw,
    act_in,
    shdown,
    mixer_out,
    expert_out,
    gate,
    up,
    down,
    disp,
    xown,
    xnbr,
    pkeep,
    psend,
    precv,
    back,
    rbuf,
    comb,
    crecv,
    rsend,
    rrecv,
    rkeep,
    stx,
    tot,
    stz,
    mwt,
    sdt,
    gall,
    sall,
    w_s,
    w_r,
    w_l,
    d_s,
    d_r,
    y_s,
    y_r,
    p_s,
    p_r,
    b_s,
    b_r,
    c_s,
    c_r,
    q_s,
    q_r,
    x_s,
    x_r,
    z_s,
    z_r,
    t_s,
    t_r,
    ag_s,
    ag_r,
    ag_ps,
    ag_pr,
):
    z, x = lax.axis_index("z"), lax.axis_index("x")
    y, c = lax.axis_index("y"), lax.axis_index("c")
    nt = 2 * ny
    nj = ny // 2
    half = xh.shape[1]
    tokens = xh.shape[0]
    par, pairs = y % 2, y // 2
    oc = 1 - c
    yn = y + 1 - 2 * par
    tp = 2 * y + c
    part = nz * ROWS
    quarter = half // 2

    def tile_of(yy, cc):
        return (yy % 2) * nt // 2 + cc * nj + yy // 2

    def tile_at(yy, cc):
        return pl.ds(pl.multiple_of(tile_of(yy, cc) * LANES, LANES), LANES)

    def rows_at(index, size):
        return pl.ds(pl.multiple_of(index * size, size), size)

    def remote(src, dst, send, recv, device):
        return pltpu.make_async_remote_copy(
            src_ref=src,
            dst_ref=dst,
            send_sem=send,
            recv_sem=recv,
            device_id=device,
            device_id_type=MESH,
        )

    def ep_peer(i):
        e = (z * nx + x + i) % (nz * nx)
        return e // nx, e % nx

    def tp_peer(i):
        t = (tp + i) % nt
        return t // 2, t % 2

    barrier = pltpu.get_barrier_semaphore()

    def greet_ep(i, _):
        zz, xx = ep_peer(i)
        pl.semaphore_signal(barrier, inc=1, device_id=(zz, xx, y, c), device_id_type=MESH)
        return _

    def greet_tp(i, _):
        yy, cc = tp_peer(i)
        pl.semaphore_signal(barrier, inc=1, device_id=(z, x, yy, cc), device_id_type=MESH)
        return _

    lax.fori_loop(1, nz * nx, greet_ep, 0)
    lax.fori_loop(1, nt, greet_tp, 0)
    pl.semaphore_wait(barrier, nz * nx - 1 + nt - 1)

    def state_x(i):
        xx = (x + i) % nx
        return remote(state, stx.at[x], x_s.at[i], x_r.at[x], (z, xx, y, c))

    def state_x_from(i):
        xx = (x + i) % nx
        return remote(state, stx.at[xx], x_s.at[i], x_r.at[xx], (z, xx, y, c))

    for i in range(1, nx):
        state_x(i).start()
    stx[x] = state[...]

    def disp_copy(g, zz):
        return remote(
            disp.at[g, rows_at(zz, ROWS)],
            xown.at[g, rows_at(z, ROWS)],
            d_s.at[g, zz],
            d_r.at[g, z],
            (zz, (x + g) % nx, y, c),
        )

    def disp_from(g, zz):
        return remote(
            disp.at[g, rows_at(z, ROWS)],
            xown.at[g, rows_at(zz, ROWS)],
            d_s.at[g, z],
            d_r.at[g, zz],
            (zz, (x + nx - g) % nx, y, c),
        )

    for g in range(nx):
        disp[g] = jnp.dot(
            pick[(x + g) % nx], xh[...], preferred_element_type=jnp.float32
        ).astype(jnp.bfloat16)

        def send(i, _, g=g):
            disp_copy(g, (z + i) % nz).start()
            return _

        lax.fori_loop(1 if g == 0 else 0, nz, send, 0)
    xown[0, rows_at(z, ROWS), :] = disp[0, rows_at(z, ROWS), :]

    width = gate_in.shape[2]
    wcol, wrow = rows_at(c, width), rows_at(c, width)
    moves = (
        (gate_in.at[0], gate.at[:, wcol]),
        (up_in.at[0], up.at[:, wcol]),
        (down_in.at[0], down.at[wrow]),
    )
    swaps = [
        remote(src, dst, w_s.at[k], w_r.at[k], (z, x, y, oc)) for k, (src, dst) in enumerate(moves)
    ]
    ocol, orow = rows_at(oc, width), rows_at(oc, width)
    froms = [
        remote(src, dst, w_s.at[k], w_r.at[k], (z, x, y, oc))
        for k, (src, dst) in enumerate(
            (
                (gate_in.at[0], gate.at[:, ocol]),
                (up_in.at[0], up.at[:, ocol]),
                (down_in.at[0], down.at[orow]),
            )
        )
    ]
    locals_ = [
        pltpu.make_async_copy(src, dst, w_l.at[k]) for k, (src, dst) in enumerate(moves)
    ]
    for copy in swaps + locals_:
        copy.start()

    mrows, srows = mixw.shape[0], shdown.shape[0]

    def tile_copies(i):
        yy, cc = tp_peer(i)
        return (
            remote(
                mixw.at[:, tile_at(yy, cc)],
                mwt.at[rows_at(tp, mrows)],
                t_s.at[0, i],
                t_r.at[0, tp],
                (z, x, yy, cc),
            ),
            remote(
                shdown.at[:, tile_at(yy, cc)],
                sdt.at[rows_at(tp, srows)],
                t_s.at[1, i],
                t_r.at[1, tp],
                (z, x, yy, cc),
            ),
        )

    def tile_from(i):
        yy, cc = tp_peer(i)
        t = 2 * yy + cc
        return (
            remote(
                mixw.at[:, tile_at(y, c)],
                mwt.at[rows_at(t, mrows)],
                t_s.at[0, i],
                t_r.at[0, t],
                (z, x, yy, cc),
            ),
            remote(
                shdown.at[:, tile_at(y, c)],
                sdt.at[rows_at(t, srows)],
                t_s.at[1, i],
                t_r.at[1, t],
                (z, x, yy, cc),
            ),
        )

    def send_tiles(i, _):
        for copy in tile_copies(i):
            copy.start()
        return _

    lax.fori_loop(1, nt, send_tiles, 0)
    mwt[rows_at(tp, mrows), :] = mixw[:, tile_at(y, c)]
    sdt[rows_at(tp, srows), :] = shdown[:, tile_at(y, c)]

    def gather_start(a, piece):
        def go(i, _):
            yy = (y + i) % ny
            remote(
                piece(y, c), piece(y, c), ag_s.at[a, i], ag_r.at[a, y], (z, x, yy, c)
            ).start()
            return _

        lax.fori_loop(1, ny, go, 0)
        remote(piece(y, c), piece(y, c), ag_ps.at[a, y], ag_pr.at[a, y], (z, x, y, oc)).start()

    def gather_forward(a, piece):
        def go(i, _):
            yy = (y + i) % ny
            remote(
                piece(y, c), piece(yy, c), ag_s.at[a, i], ag_r.at[a, yy], (z, x, yy, c)
            ).wait_recv()
            remote(
                piece(yy, c), piece(yy, c), ag_ps.at[a, yy], ag_pr.at[a, yy], (z, x, y, oc)
            ).start()
            return _

        lax.fori_loop(1, ny, go, 0)

    def gather_finish(a, piece):
        def go(yy, _):
            remote(
                piece(yy, c), piece(yy, oc), ag_ps.at[a, yy], ag_pr.at[a, yy], (z, x, y, oc)
            ).wait_recv()
            return _

        lax.fori_loop(0, ny, go, 0)

    def gather_sent(a, piece):
        def go(i, _):
            yy = (y + i) % ny
            remote(
                piece(y, c), piece(y, c), ag_s.at[a, i], ag_r.at[a, y], (z, x, yy, c)
            ).wait_send()
            return _

        def gone(yy, _):
            remote(
                piece(yy, c), piece(yy, c), ag_ps.at[a, yy], ag_pr.at[a, yy], (z, x, y, oc)
            ).wait_send()
            return _

        lax.fori_loop(1, ny, go, 0)
        lax.fori_loop(0, ny, gone, 0)

    arows = act_in.shape[0]
    channels = inside.shape[0]
    gate_piece = lambda yy, cc: gall.at[rows_at(2 * yy + cc, channels)]
    act_piece = lambda yy, cc: sall.at[rows_at(2 * yy + cc, arows)]
    mix_piece = lambda yy, cc: mixer_out.at[:, tile_at(yy, cc)]
    out_piece = lambda yy, cc: expert_out.at[:, tile_at(yy, cc)]

    sall[rows_at(tp, arows), :] = act_in[...]
    gather_start(0, act_piece)

    srow = lax.broadcasted_iota(jnp.int32, (8, KEY_DIM), 0)

    def fold(carry, item):
        mem, st = carry
        mem2, st2 = item[:channels], item[channels:]
        run, run2, dec2 = st[2:3], st2[2:3], st2[1:2]
        new = jnp.maximum(dec2 + run, run2)
        lead, tail = jnp.exp(dec2 + run - new), jnp.exp(run2 - new)
        both = lead * st + tail * st2
        both = jnp.where(srow == 1, st + st2, both)
        both = jnp.where(srow == 2, new, both)
        return lead * mem + tail * mem2, both

    def fresh(run):
        return (
            jnp.zeros((channels, KEY_DIM), jnp.float32),
            jnp.where(srow == 2, run, jnp.zeros((8, KEY_DIM), jnp.float32)),
        )

    for i in range(1, nx):
        state_x_from(i).wait_recv()
    carry = fresh(lowest)
    for i in range(nx):
        carry = fold(carry, stx[i])
    tot[:channels] = carry[0]
    tot[channels:] = carry[1]

    def state_z(zz):
        return remote(tot, stz.at[z], z_s.at[zz], z_r.at[z], (zz, x, y, c))

    def state_z_from(zz):
        return remote(tot, stz.at[zz], z_s.at[z], z_r.at[zz], (zz, x, y, c))

    def send_z(zz, _):
        state_z(zz).start()
        return _

    lax.fori_loop(z + 1, nz, send_z, 0)

    def y_copy(g):
        return remote(xown.at[g], xnbr.at[g], y_s.at[g], y_r.at[g], (z, x, yn, c))

    def p_copy(g):
        return remote(psend.at[g], precv.at[g], p_s.at[g], p_r.at[g], (z, x, yn, c))

    def back_copy(g, zz):
        return remote(
            back.at[g, rows_at(zz, ROWS)],
            rbuf.at[g, rows_at(z, ROWS)],
            b_s.at[g, zz],
            b_r.at[g, z],
            (zz, (x + nx - g) % nx, y, c),
        )

    def back_from(g, zz):
        return remote(
            back.at[g, rows_at(z, ROWS)],
            rbuf.at[g, rows_at(zz, ROWS)],
            b_s.at[g, z],
            b_r.at[g, zz],
            (zz, (x + g) % nx, y, c),
        )

    mine = pl.ds(pl.multiple_of(par * half, half), half)
    other = pl.ds(pl.multiple_of((1 - par) * half, half), half)
    skip = lambda g: jnp.where(g == 0, 1, 0)

    def step(s, acc):
        @pl.when(s < nx)
        def _():
            def wait(i, _):
                disp_from(s, (z + i) % nz).wait_recv()
                return _

            lax.fori_loop(skip(s), nz, wait, 0)
            y_copy(s).start()

        @pl.when(s == 1)
        def _():
            for copy in froms:
                copy.wait_recv()
            for copy in locals_:
                copy.wait()

        @pl.when((s >= 1) & (s <= nx))
        def _():
            g = s - 1
            y_copy(g).wait_recv()
            xa, xb = xown[g], xnbr[g]
            gv = jnp.dot(xa, gate[mine, :], preferred_element_type=jnp.float32)
            gv = gv + jnp.dot(xb, gate[other, :], preferred_element_type=jnp.float32)
            uv = jnp.dot(xa, up[mine, :], preferred_element_type=jnp.float32)
            uv = uv + jnp.dot(xb, up[other, :], preferred_element_type=jnp.float32)
            act = (gv / (1.0 + jnp.exp(-gv)) * uv).astype(jnp.bfloat16)
            psend[g] = jnp.dot(
                act, down[:, other], preferred_element_type=jnp.float32
            ).astype(jnp.bfloat16)
            p_copy(g).start()
            pkeep[g] = jnp.dot(act, down[:, mine], preferred_element_type=jnp.float32)

        @pl.when(s >= 2)
        def _():
            g = s - 2
            p_copy(g).wait_recv()
            back[g] = (pkeep[g] + precv[g].astype(jnp.float32)).astype(jnp.bfloat16)

            def send(i, _):
                back_copy(g, (z + i) % nz).start()
                return _

            lax.fori_loop(skip(g), nz, send, 0)

        return acc

    lax.fori_loop(0, nx + 2, step, 0)
    rbuf[0, rows_at(z, ROWS), :] = back[0, rows_at(z, ROWS), :]

    def from_x(i, carry):
        return fold(carry, stx[i])

    def from_z(zz, carry):
        state_z_from(zz).wait_recv()
        return fold(carry, stz[zz])

    ahead = lax.fori_loop(0, x, from_x, fresh(lowest))
    carry = lax.fori_loop(0, z, from_z, fresh(0.0))
    mem, st = fold(carry, jnp.concatenate(ahead, axis=0))
    across = lax.dot_general(
        jnp.concatenate([mem, st], axis=0),
        scaled[...].astype(jnp.float32),
        (((1,), (1,)), ((), ())),
        precision=lax.Precision.HIGHEST,
        preferred_element_type=jnp.float32,
    )
    carried = rows[0:1] + st[2:3, : rows.shape[1]]
    peak = rows[1:2]
    top = jnp.maximum(carried, peak)
    lead, tail = jnp.exp(carried - top), jnp.exp(peak - top)
    numerator = lead * across[:channels] + tail * inside[...]
    denominator = lead * across[channels : channels + 1] + tail * rows[2:3]
    hidden = numerator / jnp.maximum(jnp.abs(denominator), den_floor)
    gall[rows_at(tp, channels), :] = (hidden * sig[...]).astype(jnp.bfloat16)
    gather_start(1, gate_piece)
    gather_forward(0, act_piece)

    first = True
    for g in range(nx):

        def wait(i, _, g=g):
            back_from(g, (z + i) % nz).wait_recv()
            return _

        lax.fori_loop(1 if g == 0 else 0, nz, wait, 0)
        xx = (x + g) % nx
        dims = (((0,), (0,)), ((), ()))
        got = rbuf[g]
        add = lax.dot_general(whi[xx], got, dims, preferred_element_type=jnp.float32)
        add = add + lax.dot_general(wlo[xx], got, dims, preferred_element_type=jnp.float32)
        comb[...] = add if g == 0 else comb[...] + add
        if g == 0:
            gather_forward(1, gate_piece)

            def wait_tiles(i, _):
                for copy in tile_from(i):
                    copy.wait_recv()
                return _

            lax.fori_loop(1, nt, wait_tiles, 0)
            gather_finish(1, gate_piece)
            mixer_out[:, tile_at(y, c)] = lax.dot_general(
                gall[...], mwt[...], dims, preferred_element_type=jnp.float32
            ).astype(jnp.bfloat16)
            gather_start(2, mix_piece)

    keep = pl.ds(pl.multiple_of(c * quarter, quarter), quarter)
    give = pl.ds(pl.multiple_of(oc * quarter, quarter), quarter)
    core_swap = remote(comb.at[:, give], crecv, c_s, c_r, (z, x, y, oc))
    core_swap.start()
    gather_finish(0, act_piece)
    shared = lax.dot_general(
        sall[...], sdt[...], (((0,), (0,)), ((), ())), preferred_element_type=jnp.float32
    )
    core_swap.wait_recv()
    kept = comb[:, keep] + crecv[...]
    for j in range(nj):
        piece = kept[:, j * LANES : (j + 1) * LANES]
        rkeep[j] = piece
        rsend[j] = piece.astype(jnp.bfloat16)

    def reduce_copy(i):
        j = (pairs + i) % nj
        return remote(
            rsend.at[j], rrecv.at[pairs], q_s.at[i], q_r.at[pairs], (z, x, 2 * j + par, c)
        )

    def reduce_from(i):
        j = (pairs + i) % nj
        return remote(rsend.at[j], rrecv.at[j], q_s.at[i], q_r.at[j], (z, x, 2 * j + par, c))

    for i in range(1, nj):
        reduce_copy(i).start()
    gather_forward(2, mix_piece)
    result = rkeep[pairs] + shared
    for i in range(1, nj):
        reduce_from(i).wait_recv()
        result = result + rrecv[(pairs + i) % nj].astype(jnp.float32)
    expert_out[:, tile_at(y, c)] = result.astype(jnp.bfloat16)
    gather_start(3, out_piece)
    gather_finish(2, mix_piece)
    gather_forward(3, out_piece)
    gather_finish(3, out_piece)

    for i in range(1, nx):
        state_x(i).wait_send()
    for g in range(nx):

        def gone(i, _, g=g):
            zz = (z + i) % nz
            disp_copy(g, zz).wait_send()
            back_copy(g, zz).wait_send()
            return _

        lax.fori_loop(1 if g == 0 else 0, nz, gone, 0)
        y_copy(g).wait_send()
        p_copy(g).wait_send()
    for copy in swaps:
        copy.wait_send()

    def tiles_gone(i, _):
        for copy in tile_copies(i):
            copy.wait_send()
        return _

    def z_gone(zz, _):
        state_z(zz).wait_send()
        return _

    lax.fori_loop(1, nt, tiles_gone, 0)
    lax.fori_loop(z + 1, nz, z_gone, 0)
    core_swap.wait_send()
    for i in range(1, nj):
        reduce_copy(i).wait_send()
    for a, piece in enumerate((act_piece, gate_piece, mix_piece, out_piece)):
        gather_sent(a, piece)


def shards(
    nz,
    nx,
    ny,
    queries,
    key_vectors,
    values,
    out_gate,
    input_gate,
    forget_gate,
    mix_weight,
    expert_input,
    norm_gain,
    route_ids,
    route_weights,
    expert_gate,
    expert_up,
    expert_down,
    shared_gate,
    shared_up,
    shared_down,
):
    y, c = lax.axis_index("y"), lax.axis_index("c")
    tokens, width = expert_input.shape
    half = width // 2
    length = queries.shape[0]
    channels = values.shape[1]
    head = (2 * y + c) // (2 * ny // MEMORY_HEADS)
    state, rows, inside, sig, scaled = mixer_local(
        queries, key_vectors, values, out_gate, input_gate, forget_gate, head
    )
    wide = expert_input.astype(jnp.float32)
    normed = (
        wide
        * lax.rsqrt(jnp.mean(wide * wide, axis=-1, keepdims=True) + epsilon)
        * norm_gain
    ).astype(jnp.bfloat16)
    xh = lax.dynamic_slice_in_dim(normed, (y % 2) * half, half, 1)
    pick, whi, wlo = routing(route_ids, route_weights, y // (ny // 2), c, nz, nx)
    dims = (((0,), (1,)), ((), ()))
    sg = lax.dot_general(shared_gate, normed, dims, preferred_element_type=jnp.float32)
    su = lax.dot_general(shared_up, normed, dims, preferred_element_type=jnp.float32)
    act = (jax.nn.silu(sg) * su).astype(jnp.bfloat16)

    units = expert_gate.shape[2]
    part = nz * ROWS
    nj = ny // 2
    nt = 2 * ny
    vmem = pl.BlockSpec(memory_space=pltpu.VMEM)
    hbm = pl.BlockSpec(memory_space=pl.ANY)
    dma = pltpu.SemaphoreType.DMA
    bf, f32 = jnp.bfloat16, jnp.float32
    return pl.pallas_call(
        functools.partial(kernel, nz, nx, ny),
        out_shape=(
            jax.ShapeDtypeStruct((length, width), bf),
            jax.ShapeDtypeStruct((tokens, width), bf),
        ),
        in_specs=[vmem] * 4 + [hbm] * 3 + [vmem] * 8,
        out_specs=(vmem, vmem),
        scratch_shapes=[
            pltpu.VMEM((width, 2 * units), bf),
            pltpu.VMEM((width, 2 * units), bf),
            pltpu.VMEM((2 * units, width), bf),
            pltpu.VMEM((nx, part, half), bf),
            pltpu.VMEM((nx, part, half), bf),
            pltpu.VMEM((nx, part, half), bf),
            pltpu.VMEM((nx, part, half), f32),
            pltpu.VMEM((nx, part, half), bf),
            pltpu.VMEM((nx, part, half), bf),
            pltpu.VMEM((nx, part, half), bf),
            pltpu.VMEM((nx, part, half), bf),
            pltpu.VMEM((tokens, half), f32),
            pltpu.VMEM((tokens, half // 2), f32),
            pltpu.VMEM((nj, tokens, LANES), bf),
            pltpu.VMEM((nj, tokens, LANES), bf),
            pltpu.VMEM((nj, tokens, LANES), f32),
            pltpu.VMEM((nx, channels + 8, KEY_DIM), f32),
            pltpu.VMEM((channels + 8, KEY_DIM), f32),
            pltpu.VMEM((nz, channels + 8, KEY_DIM), f32),
            pltpu.VMEM((nt * channels, LANES), bf),
            pltpu.VMEM((nt * shared_down.shape[0], LANES), bf),
            pltpu.VMEM((nt * channels, length), bf),
            pltpu.VMEM((nt * shared_down.shape[0], tokens), bf),
            dma((3,)),
            dma((3,)),
            dma((3,)),
            dma((nx, nz)),
            dma((nx, nz)),
            dma((nx,)),
            dma((nx,)),
            dma((nx,)),
            dma((nx,)),
            dma((nx, nz)),
            dma((nx, nz)),
            dma,
            dma,
            dma((nj,)),
            dma((nj,)),
            dma((nx,)),
            dma((nx,)),
            dma((nz,)),
            dma((nz,)),
            dma((2, nt)),
            dma((2, nt)),
            dma((4, ny)),
            dma((4, ny)),
            dma((4, ny)),
            dma((4, ny)),
        ],
        compiler_params=pltpu.CompilerParams(
            collective_id=0, has_side_effects=True, vmem_limit_bytes=50 * 1024 * 1024
        ),
        name="exchange",
    )(
        xh,
        pick,
        whi,
        wlo,
        expert_gate,
        expert_up,
        expert_down,
        state,
        rows,
        inside,
        sig,
        scaled,
        mix_weight,
        act,
        shared_down,
    )


def solution(mesh):
    count, nt = mesh.shape["ep"], mesh.shape["tp"]
    nx = 4 if count % 16 == 0 else 2
    nz, ny = count // nx, nt // 2
    finer = Mesh(mesh.devices.reshape(nz, nx, ny, 2), ("z", "x", "y", "c"))
    placed = (
        P(EP, None),
        P(EP, None),
        P(EP, TP),
        P(EP, TP),
        P(EP, None),
        P(EP, None),
        P(TP, None),
        P(EP, None),
        P(),
        P(EP, None),
        P(EP, None),
        P(EP + TP, None, None),
        P(EP + TP, None, None),
        P(EP + TP, None, None),
        P(None, TP),
        P(None, TP),
        P(TP, None),
    )
    return jax.shard_map(
        functools.partial(shards, nz, nx, ny),
        mesh=finer,
        in_specs=placed,
        out_specs=(P(EP, None), P(EP, None)),
        check_vma=False,
    )
```

time: 428 us -> 135 us (0.32)
  blocking collectives: 186 us -> 0 us
  Pallas kernels: 0 us -> 120 us
  waiting for transfers between devices: 64.6 us -> 0 us
  between operations: 49.7 us -> 1.01 us
  local copies, waits for them, and re-layouts: 54.5 us -> 6.03 us
  starting transfers between devices: 26.2 us -> 0 us
  other arithmetic: 27.8 us -> 6.82 us
  matrix products: 17.5 us -> 1.69 us
    pallas_call x0 -> x1, Pallas kernels: none -> 120 us  [shards(): pl.pallas_call(functools.partial(kernel, nz, nx, ny), out_shape=(jax.Shap...]
    all_to_all x1 -> x0, blocking collectives: 107 us -> none  [expert_half(): lax.all_to_all(outgoing, EP, split_axis=0, concat_axis=0, tiled=True)]
    all_gather x3 -> x0, blocking collectives: 79 us -> none  [the longest x2 41.1 us: all_in_one(): both, at, found = (lax.all_gather(jnp.concatenate(lines), axis), 0, {})]
    all_to_all x3 -> x0, waiting for transfers between devices: 64.6 us -> none  [the longest x1 48.3 us: expert_half(): lax.all_to_all(partial_value, EP, split_axis=0, concat_axis=0, tiled=True)]
    gather x5 -> x0, local copies, waits for them, and re-layouts: 29.9 us -> none  [the longest x4 23.9 us: expert_half(): flat_back[gather_at[:, pick_index]].astype(jnp.float32)]
    all_to_all x3 -> x0, starting transfers between devices: 26.2 us -> none  [the longest x1 16 us: summed_on_arrival(): lax.all_to_all(blocks, axis, split_axis=0, concat_axis=0, tiled=True)]
    another operation x4 -> x0, other arithmetic: 18.5 us -> none
    dot_general x9 -> x6, matrix products: 17.5 us -> 1.69 us  [the longest x1 0.43 us: shards(): lax.dot_general(shared_up, normed, dims, preferred_element_type=jnp.float32)]
  transfers between devices with their start and end apart: 4 -> 0, of which waited for: 2 -> 0; matrix products, arithmetic and copies ran while one was open for 4% -> 0% of each run, Pallas kernels for 0% -> 0%
where the time goes in v1:
time: 135 us
  Pallas kernels  120 us (89%)
  other arithmetic  6.82 us (5%)
  local copies, waits for them, and re-layouts  6.03 us (4%)
  matrix products  1.69 us (1%)
    pallas_call x1, Pallas kernels, shards(): pl.pallas_call(functools.partial(kernel, nz, nx, ny), out_shape=(jax.Shap...  120 us
    unnamed x34, local copies, waits for them, and re-layouts  3.87 us

profile of v1, /device:TPU:1, one launch (start us, length us, event | category | flops | bytes accessed | tf_op | source)
XLA Modules:
  0.0 135.1 jit_solution(7752126451473809804)
XLA Ops:
  0.8 0.1 pad.3.clone
  0.8 0.8 select_reduce_fusion.2
  1.7 0.1 select_reduce_fusion
  1.8 0.6 slice.35
  2.4 1.2 fusion.34
  3.6 1.3 subtract_exponential_fusion
  4.9 0.1 fusion.14
  5.0 0.7 broadcast_in_dim.152
  5.7 0.6 broadcast_in_dim.153
  6.3 0.9 fusion.12
  7.3 1.5 %fusion = f32[256]{0:T(256)S(1)} fusion(bf16[256,2048]{1,0:T(8,128)(2,1)} %param.24), kind=kLoop, calls=%fused_computation.2 | loop fusion | flops 1572608 | bytes 1049600 | tf_op jit(solution)/shard_map/reduce_sum | solution.py:695
  8.8 0.1 eq.131
  9.0 0.1 select_add_fusion
  9.1 0.3 fusion.6
  9.4 0.2 fusion.37
  9.6 0.1 maximum_maximum_fusion.rows
  9.7 0.1 convolution_bitcast_fusion.1.inside
  9.8 0.3 convolution_bitcast_fusion
  10.2 0.1 fusion.9.pick
  10.3 0.2 fusion.8
  10.5 0.3 fusion.2
  10.8 0.4 convolution_bitcast_fusion.3
  11.2 0.5 copy-done.8
  11.7 0.4 fusion.7.act_in
  12.2 0.5 copy-done.1
  12.7 0.2 copy-done.2
  12.9 0.2 copy-done.3
  13.1 0.1 copy-done.4
  13.2 119.5 %exchange.1 = (bf16[128,2048]{1,0:T(8,128)(2,1)S(1)}, bf16[256,2048]{1,0:T(8,128)(2,1)}) custom-call(bf16[256,1024]{1,0:T(8,128)(2,1)S(1)} %constant_dynamic-slice_fusion.xh, bf16[4,128,256]{2,1,0:T(8,128)(2,1)S(1)} %fusion.9.pick, bf16[4,128,256]{2,1,0:T(8,128)(2,1)S(1)} %get-tuple-element.5.whi, bf16[4,128,256]{2,1,0:T(8,128)(2,1)S(1)} %get-tuple-element.4.wlo, ...), custom_call_target="tpu_custom_call" | custom-call | tf_op jit(solution)/shard_map/exchange/pallas_call | solution.py:713
  132.7 0.8 copy.22
  133.5 0.6 copy-done.7
  134.1 1.0 copy.23
  (43 shorter events, 0.3 us)
Async XLA Ops:
  0.6 10.2 %copy-start = (bf16[2048,32]{0,1:T(8,128)(2,1)S(1)}, bf16[2048,32]{0,1:T(8,128)(2,1)}, u32[]{:S(2)}) copy-start(bf16[2048,32]{0,1:T(8,128)(2,1)} %param.31) | copy-start | bytes 393220
  0.6 8.8 %copy-start.9 = (bf16[128,512]{1,0:T(8,128)(2,1)S(1)}, bf16[128,512]{1,0:T(8,128)(2,1)}, u32[]{:S(2)}) copy-start(bf16[128,512]{1,0:T(8,128)(2,1)} %param.18) | copy-start | bytes 393220
  0.7 8.8 %copy-start.11 = (bf16[128,512]{1,0:T(8,128)(2,1)S(1)}, bf16[128,512]{1,0:T(8,128)(2,1)}, u32[]{:S(2)}) copy-start(bf16[128,512]{1,0:T(8,128)(2,1)} %param.17) | copy-start | bytes 393220
  0.7 8.3 %copy-start.15 = (f32[256,4]{0,1:T(4,128)S(1)}, f32[256,4]{0,1:T(4,128)}, u32[]{:S(2)}) copy-start(f32[256,4]{0,1:T(4,128)} %param.27) | copy-start | bytes 12292
  0.7 8.2 %copy-start.14 = (s32[256,4]{0,1:T(4,128)S(1)}, s32[256,4]{0,1:T(4,128)}, u32[]{:S(2)}) copy-start(s32[256,4]{0,1:T(4,128)} %param.26) | copy-start | bytes 12292
  0.7 8.7 %copy-start.12 = (bf16[128,64]{0,1:T(8,128)(2,1)S(1)}, bf16[128,64]{0,1:T(8,128)(2,1)}, u32[]{:S(2)}) copy-start(bf16[128,64]{0,1:T(8,128)(2,1)} %param.20) | copy-start | bytes 49156
  6.3 3.4 %copy-start.10 = (bf16[128,64]{0,1:T(8,128)(2,1)S(1)}, bf16[128,64]{0,1:T(8,128)(2,1)}, u32[]{:S(2)}) copy-start(bf16[128,64]{0,1:T(8,128)(2,1)} %param.19) | copy-start | bytes 49156
  9.0 1.4 %copy-start.6 = (bf16[256,2048]{1,0:T(8,128)(2,1)S(1)}, bf16[256,2048]{1,0:T(8,128)(2,1)}, u32[]{:S(2)}) copy-start(bf16[256,2048]{1,0:T(8,128)(2,1)} %param.24) | copy-start | bytes 3145732
  9.1 1.4 %copy-start.13 = (f32[2048]{0:T(1024)S(1)}, f32[2048]{0:T(1024)}, u32[]{:S(2)}) copy-start(f32[2048]{0:T(1024)} %param.25) | copy-start | bytes 24580
  10.8 0.9 copy-start.8
  11.7 1.0 copy-start.1
  11.7 1.2 copy-start.2
  11.7 1.4 %copy-start.3 = (bf16[1,128,2048]{2,1,0:T(8,128)(2,1)S(1)}, bf16[1,128,2048]{2,1,0:T(8,128)(2,1)}, u32[]{:S(2)}) copy-start(bf16[1,128,2048]{2,1,0:T(8,128)(2,1)} %down_in.1) | copy-start | bytes 1572868
  11.7 1.4 %copy-start.4 = (bf16[64,2048]{1,0:T(8,128)(2,1)S(1)}, bf16[64,2048]{1,0:T(8,128)(2,1)}, u32[]{:S(2)}) copy-start(bf16[64,2048]{1,0:T(8,128)(2,1)} %mixw.1) | copy-start | bytes 786436
  11.7 1.4 %copy-start.5 = (bf16[32,2048]{1,0:T(8,128)(2,1)S(1)}, bf16[32,2048]{1,0:T(8,128)(2,1)}, u32[]{:S(2)}) copy-start(bf16[32,2048]{1,0:T(8,128)(2,1)} %shdown.1) | copy-start | bytes 393220
  132.7 1.4 %copy-start.7 = (bf16[256,2048]{1,0:T(8,128)(2,1)S(1)}, bf16[256,2048]{1,0:T(8,128)(2,1)}, u32[]{:S(2)}) copy-start(bf16[256,2048]{1,0:T(8,128)(2,1)} %get-tuple-element.21) | copy-start | bytes 3145732
